TPU v7x, 32 devices: a whole 2x2x4 slice. The times are simulated.
32 devices in a mesh: sp: 4 (over y, x), tp: 8 (over z, core).
Axes of the slice: x: 2, y: 2, z: 4, core: 2. Of those that a mesh axis runs over, the one named last changes fastest.
Arguments:
- query_rows: bfloat16 [8192, 1024], P('sp', 'tp'), may hold values from -6 to 6
- key_rows: bfloat16 [8192, 1024], P('sp', 'tp'), may hold values from -6 to 6
- value_rows: bfloat16 [8192, 1024], P('sp', 'tp'), may hold values from -6 to 6
- gate_rows: bfloat16 [8192, 1024], P('sp', 'tp'), may hold values from -6 to 6
- log_decay: float32 [16, 8192], P('tp', 'sp'), may hold values from -1 to 0
- residual: bfloat16 [8192, 2048], P(('sp', 'tp')), may hold values from -6 to 6
- head_gain: float32 [1024], P('tp'), may hold values from 0.1 to 1.9
- out_weight: bfloat16 [1024, 2048], P(None, 'tp'), may hold values from -0.1875 to 0.1875
- norm_gain: float32 [2048], replicated, may hold values from 0.1 to 1.9
- expert_ids: int32 [8192, 2], P(('sp', 'tp')), may hold values from 0 to 3, all different within a row; in each aligned block of 256 rows (0 to 255, 256 to 511, ...) at most 192 rows name the same one
- route_weights: float32 [8192, 2], P(('sp', 'tp')), may hold values from 0.2 to 1
- expert_gate: bfloat16 [2048, 4096], P(None, ('sp', 'tp')), may hold values from -0.125 to 0.125
- expert_up: bfloat16 [2048, 4096], P(None, ('sp', 'tp')), may hold values from -0.125 to 0.125
- expert_down: bfloat16 [2048, 4096], P(None, ('sp', 'tp')), may hold values from -0.1875 to 0.1875
- shared_gate: bfloat16 [2048, 512], replicated, may hold values from -0.125 to 0.125
- shared_up: bfloat16 [2048, 512], replicated, may hold values from -0.125 to 0.125
- shared_down: bfloat16 [2048, 512], replicated, may hold values from -0.25 to 0.25
Outputs:
- result: bfloat16 [8192, 2048], P(('sp', 'tp'))
Inputs may be any that keep to these rules, and one draw needn't show every extreme that they name: `expert_ids`: each row names 2 different experts. Within the rows of one device (aligned blocks of 256 rows) no expert is named by more than 192 rows, and in some block an expert is named by exactly 192 rows.
All inputs are finite; a program needn't handle non-finite values.
Results may differ from a plain program's by a relative error of at most 0.0075.
Values may be sent and summed in bfloat16 or wider, within the bound.
A program may use at most 128 MiB of HBM per device.

v0:
```python
import jax
import jax.numpy as jnp
from jax import lax
from jax.sharding import PartitionSpec as P

HEAD = 64
SPAN = 512
eps = 1e-05


def entering(value, axis, join, neutral):
    count, mine = (lax.axis_size(axis), lax.axis_index(axis))
    pieces = jax.tree.map(lambda part: lax.all_gather(part, axis), value)
    so_far = jax.tree.map(
        lambda part, zero: jnp.full_like(part, 0) + jnp.asarray(zero, part.dtype), value, neutral
    )

    def hop(position, so_far):
        longer = join(so_far, jax.tree.map(lambda part: part[position], pieces))
        return jax.tree.map(lambda new, old: jnp.where(position < mine, new, old), longer, so_far)

    return lax.fori_loop(0, count - 1, hop, so_far)


def block_pass(queries, key_heads, values, log_decay, state):
    rows, heads, width = queries.shape
    count = rows // SPAN
    scale = width ** (-0.5)
    query_blocks = queries.reshape(count, SPAN, heads, width)
    key_blocks = key_heads.reshape(count, SPAN, heads, width)
    value_blocks = values.reshape(count, SPAN, heads, width)
    decay_blocks = log_decay.reshape(heads, count, SPAN).transpose(1, 0, 2)
    offsets = jnp.arange(SPAN, dtype=jnp.int32)
    causal = offsets[:, None] >= offsets[None, :]

    def advance(carry, inputs):
        block_queries, block_keys, block_values, decay_block = inputs
        running = jnp.cumsum(decay_block, axis=1)
        spread = running[:, :, None] - running[:, None, :]
        damping = jnp.exp(jnp.where(causal[None], spread, -jnp.inf))
        attention_scores = jnp.einsum(
            "xru,jru->rxj", block_queries, block_keys, preferred_element_type=jnp.float32
        )
        decay_weighted = (attention_scores * scale * damping).astype(jnp.bfloat16)
        inner_block_term = jnp.einsum(
            "svc,csj->vsj", decay_weighted, block_values, preferred_element_type=jnp.float32
        )
        carried = jnp.einsum(
            "nhd,hde->nhe",
            block_queries.astype(jnp.float32),
            carry,
            precision=lax.Precision.HIGHEST,
        )
        carried = carried * jnp.exp(running).T[:, :, None]
        decay_to_block_end = jnp.exp(running[:, -1:] - running).T[:, :, None] * scale
        state_update = jnp.einsum(
            "jok,jow->okw",
            block_keys.astype(jnp.float32) * decay_to_block_end,
            block_values.astype(jnp.float32),
            precision=lax.Precision.HIGHEST,
        )
        carry = carry * jnp.exp(running[:, -1])[:, None, None] + state_update
        return (carry, inner_block_term + carried)

    final, outputs = lax.scan(
        advance, state, (query_blocks, key_blocks, value_blocks, decay_blocks)
    )
    return (final, outputs.reshape(rows, heads, width))


def combine_states(earlier, later):
    return (earlier[0] * later[0], earlier[1] * later[0][:, None, None] + later[1])


def entering_state(totals, own_state):
    identity = (jnp.ones_like(totals), jnp.zeros_like(own_state))
    return entering((totals, own_state), "sp", combine_states, identity)[1]


def on_device(
    query_rows,
    key_rows,
    value_rows,
    gate_rows,
    log_decay,
    residual,
    head_gain,
    out_weight,
    norm_gain,
    expert_ids,
    route_weights,
    expert_gate,
    expert_up,
    expert_down,
    shared_gate,
    shared_up,
    shared_down,
):
    seq_rows, local_width = query_rows.shape
    heads = local_width // HEAD
    out_full, gate_full, up_full, down_full = (
        lax.all_gather(out_weight, "tp", axis=1, tiled=True),
        lax.all_gather(expert_gate, "tp", axis=1, tiled=True),
        lax.all_gather(expert_up, "tp", axis=1, tiled=True),
        lax.all_gather(expert_down, "tp", axis=1, tiled=True),
    )
    queries = query_rows.reshape(seq_rows, heads, HEAD)
    key_heads = key_rows.reshape(seq_rows, heads, HEAD)
    values = value_rows.reshape(seq_rows, heads, HEAD)
    zero_state = jnp.zeros((heads, HEAD, HEAD), jnp.float32)
    running = jnp.cumsum(log_decay, axis=1)
    totals = jnp.exp(running[:, -1])
    own_state, retained = block_pass(queries, key_heads, values, log_decay, zero_state)
    incoming = entering_state(totals, own_state)
    readout = jnp.einsum(
        "nhd,hde->nhe", queries.astype(jnp.float32), incoming, precision=lax.Precision.HIGHEST
    )
    retained = retained + readout * jnp.exp(running).T[:, :, None]
    centered = retained - jnp.mean(retained, axis=2, keepdims=True)
    normed = centered * lax.rsqrt(jnp.mean(centered * centered, axis=2, keepdims=True) + eps)
    ret_rows = (
        normed.reshape(seq_rows, local_width)
        * head_gain
        * jax.nn.silu(gate_rows.astype(jnp.float32))
    ).astype(jnp.bfloat16)
    token_rows = lax.all_to_all(ret_rows, "tp", split_axis=0, concat_axis=1, tiled=True)
    mixer = jnp.dot(token_rows, out_full, preferred_element_type=jnp.float32)
    hidden = (residual.astype(jnp.float32) + mixer).astype(jnp.bfloat16)
    hidden_wide = hidden.astype(jnp.float32)
    normed_rows = (
        hidden_wide
        * lax.rsqrt(jnp.mean(hidden_wide * hidden_wide, axis=1, keepdims=True) + eps)
        * norm_gain
    ).astype(jnp.bfloat16)
    shared_mid = (
        jax.nn.silu(jnp.dot(normed_rows, shared_gate, preferred_element_type=jnp.float32))
        * jnp.dot(normed_rows, shared_up, preferred_element_type=jnp.float32)
    ).astype(jnp.bfloat16)
    shared_out = lax.dot_general(
        shared_mid, shared_down, (((1,), (1,)), ((), ())), preferred_element_type=jnp.float32
    )
    specialist_networks = lax.axis_size("sp")
    token_count, chosen_count = expert_ids.shape
    model_width = normed_rows.shape[1]
    capacity = 3 * token_count * chosen_count // (2 * specialist_networks)
    flat_ids = expert_ids.reshape(-1)
    matches = (
        flat_ids[:, None] == jnp.arange(specialist_networks, dtype=jnp.int32)[None, :]
    ).astype(jnp.int32)
    position = jnp.sum((jnp.cumsum(matches, axis=0) - 1) * matches, axis=1)
    slot = flat_ids * capacity + position
    owner = jnp.arange(token_count * chosen_count, dtype=jnp.int32) // chosen_count
    slot_token = jnp.zeros((specialist_networks * capacity,), jnp.int32).at[slot].set(owner)
    slot_live = jnp.zeros((specialist_networks * capacity,), jnp.bfloat16).at[slot].set(1.0)
    outgoing = (normed_rows[slot_token] * slot_live[:, None]).reshape(
        specialist_networks, capacity, model_width
    )
    arrived = lax.all_to_all(outgoing, "sp", split_axis=0, concat_axis=0, tiled=True)
    flat_rows = arrived.reshape(-1, model_width)
    middle = (
        jax.nn.silu(jnp.dot(flat_rows, gate_full, preferred_element_type=jnp.float32))
        * jnp.dot(flat_rows, up_full, preferred_element_type=jnp.float32)
    ).astype(jnp.bfloat16)
    outcome = lax.dot_general(
        middle, down_full, (((1,), (1,)), ((), ())), preferred_element_type=jnp.float32
    ).astype(jnp.bfloat16)
    processed = outcome.reshape(arrived.shape)
    returned = lax.all_to_all(processed, "sp", split_axis=0, concat_axis=0, tiled=True)
    picked = returned.reshape(specialist_networks * capacity, model_width)[slot].astype(jnp.float32)
    decay_weighted = picked * route_weights.reshape(-1)[:, None]
    routed = jnp.sum(decay_weighted.reshape(token_count, chosen_count, model_width), axis=1)
    return (hidden_wide + routed + shared_out).astype(jnp.bfloat16)


def solution(mesh):
    placed = (
        P("sp", "tp"),
        P("sp", "tp"),
        P("sp", "tp"),
        P("sp", "tp"),
        P("tp", "sp"),
        P(("sp", "tp"), None),
        P("tp"),
        P(None, "tp"),
        P(),
        P(("sp", "tp"), None),
        P(("sp", "tp"), None),
        P(None, ("sp", "tp")),
        P(None, ("sp", "tp")),
        P(None, ("sp", "tp")),
        P(),
        P(),
        P(),
    )
    return jax.shard_map(
        on_device, mesh=mesh, in_specs=placed, out_specs=P(("sp", "tp"), None), check_vma=False
    )
```

profile of v0, /device:TPU:0, one launch (start us, length us, event | category | flops | bytes accessed | tf_op | source)
XLA Modules:
  0.0 303.6 jit_solution(6103581982348177756)
XLA Ops:
  6.5 0.7 all-gather.7.cloned.1.call-update
  7.3 0.7 all-gather.9.cloned.1.call-update
  8.1 0.7 all-gather.11.cloned.1.call-update
  11.2 2.4 reshape.235
  15.0 2.1 copy.71
  17.1 11.4 %all-reduce = f32[8]{0:T(128)S(1)} all-reduce(f32[8]{0:T(128)S(1)} %bitcast_dynamic-update-slice_fusion), channel_id=2, replica_groups=mesh['sp'=4,'tp'=8] {'sp'}, use_global_device_ids=true, to_apply=%add | all-reduce | flops 8 | bytes 64
  28.4 0.7 reshape.222
  29.1 3.2 %reshape.233 = bf16[4,512,2,64]{3,2,1,0:T(2,128)(2,1)} reshape(bf16[2048,128]{1,0:T(8,128)(2,1)} %param.22) | data formatting | bytes 1048576 | tf_op jit(solution)/shard_map/reshape;reshape | solution.py:30
  32.3 3.5 %copy.66 = bf16[4,512,2,64]{1,3,2,0:T(8,128)(2,1)} copy(bf16[4,512,2,64]{3,2,1,0:T(2,128)(2,1)} %reshape.233) | data formatting | bytes 1048576
  35.8 3.2 %reshape.234 = bf16[4,512,2,64]{3,2,1,0:T(2,128)(2,1)} reshape(bf16[2048,128]{1,0:T(8,128)(2,1)} %param.23) | data formatting | bytes 1048576 | tf_op jit(solution)/shard_map/reshape;reshape | solution.py:31
  39.0 3.5 %copy.67 = bf16[4,512,2,64]{1,3,2,0:T(8,128)(2,1)} copy(bf16[4,512,2,64]{3,2,1,0:T(2,128)(2,1)} %reshape.234) | data formatting | bytes 1048576
  42.5 1.8 copy.68
  44.3 50.0 %while.27 = (s32[]{:T(128)}, f32[2,64,64]{2,1,0:T(8,128)S(1)}, f32[4,512,2,64]{1,0,3,2:T(4,128)}, f32[4,2,512]{2,1,0:T(2,128)S(1)}, bf16[4,512,2,64]{1,3,2,0:T(8...) while((s32[]{:T(128)}, f32[2,64,64]{2,1,0:T(8,128)S(1)}, ...), condition=%wide.region_3.4_spmd.clone, body=%wide.region_0.3_spmd.clone.sunk | while | flops 238192672 | bytes 3317096 | solution.py:65
  44.3 0.6 reduce-window.38
  45.7 2.1 fusion.108
  47.8 1.2 fusion.109
  49.3 6.2 %dynamic_update_slice.6 = f32[4,512,2,64]{1,0,3,2:T(4,128)} dynamic-update-slice(f32[4,512,2,64]{1,0,3,2:T(4,128)} %get-tuple-element.330, f32[1,512,2,64]{1,0,3,2:T(1,128)S(1)} %copy.122, s32[]{:T(128)} %get-tuple-element.328, s32[]{:T(128)} %constant.94.clone.1..sunk, s32[]{:T(128)} %constant.94.clone.1..sunk, s32[]{:T(128)} %constant.94.clone.1..sunk) | dynamic-update-slice | bytes 524292 | tf_op jit(solution)/shard_map/while/body/jit(dynamic_update_index_in_dim)/dynamic_update_slice | solution.py:65
  55.5 1.2 convolution_add_fusion.4
  56.8 0.6 reduce-window.38
  58.2 2.2 fusion.108
  60.4 1.2 fusion.109
  61.9 6.2 %dynamic_update_slice.6 = f32[4,512,2,64]{1,0,3,2:T(4,128)} dynamic-update-slice(f32[4,512,2,64]{1,0,3,2:T(4,128)} %get-tuple-element.330, f32[1,512,2,64]{1,0,3,2:T(1,128)S(1)} %copy.122, s32[]{:T(128)} %get-tuple-element.328, s32[]{:T(128)} %constant.94.clone.1..sunk, s32[]{:T(128)} %constant.94.clone.1..sunk, s32[]{:T(128)} %constant.94.clone.1..sunk) | dynamic-update-slice | bytes 524292 | tf_op jit(solution)/shard_map/while/body/jit(dynamic_update_index_in_dim)/dynamic_update_slice | solution.py:65
  68.1 1.3 convolution_add_fusion.4
  69.4 0.6 reduce-window.38
  70.7 2.1 fusion.108
  72.9 1.2 fusion.109
  74.4 6.1 %dynamic_update_slice.6 = f32[4,512,2,64]{1,0,3,2:T(4,128)} dynamic-update-slice(f32[4,512,2,64]{1,0,3,2:T(4,128)} %get-tuple-element.330, f32[1,512,2,64]{1,0,3,2:T(1,128)S(1)} %copy.122, s32[]{:T(128)} %get-tuple-element.328, s32[]{:T(128)} %constant.94.clone.1..sunk, s32[]{:T(128)} %constant.94.clone.1..sunk, s32[]{:T(128)} %constant.94.clone.1..sunk) | dynamic-update-slice | bytes 524292 | tf_op jit(solution)/shard_map/while/body/jit(dynamic_update_index_in_dim)/dynamic_update_slice | solution.py:65
  80.5 1.2 convolution_add_fusion.4
  81.8 0.6 reduce-window.38
  83.2 2.1 fusion.108
  85.3 1.2 fusion.109
  86.9 6.1 %dynamic_update_slice.6 = f32[4,512,2,64]{1,0,3,2:T(4,128)} dynamic-update-slice(f32[4,512,2,64]{1,0,3,2:T(4,128)} %get-tuple-element.330, f32[1,512,2,64]{1,0,3,2:T(1,128)S(1)} %copy.122, s32[]{:T(128)} %get-tuple-element.328, s32[]{:T(128)} %constant.94.clone.1..sunk, s32[]{:T(128)} %constant.94.clone.1..sunk, s32[]{:T(128)} %constant.94.clone.1..sunk) | dynamic-update-slice | bytes 524292 | tf_op jit(solution)/shard_map/while/body/jit(dynamic_update_index_in_dim)/dynamic_update_slice | solution.py:65
  93.0 1.2 convolution_add_fusion.4
  94.3 8.0 %all-gather.1 = f32[8,64,64]{2,1,0:T(8,128)S(1)} all-gather(f32[2,64,64]{2,1,0:T(8,128)S(1)} %get-tuple-element.143), channel_id=3, replica_groups=mesh['sp'=4,'tp'=8] {'sp'}, dimensions={0}, use_global_device_ids=true | all-gather | bytes 163840 | tf_op jit(solution)/shard_map/all_gather | solution.py:13
  102.3 2.3 while.28
  102.3 0.7 dynamic-slice_bitcast_fusion.2
  103.1 0.7 dynamic-slice_bitcast_fusion.2
  103.8 0.7 dynamic-slice_bitcast_fusion.2
  104.6 1.9 reshape.180
  106.5 1.7 fusion.73
  108.5 1.1 subtract_multiply_fusion
  109.6 1.6 copy.73
  111.2 2.2 fusion.54
  113.3 4.8 %all-to-all-start = ((bf16[8,256,128]{2,1,0:T(8,128)(2,1)}), bf16[8,256,128]{2,1,0:T(8,128)(2,1)S(1)}, u32[]{:S(2)}, u32[]{:S(2)}) async-start(bf16[8,256,128]{2,1,0:T(8,128)(2,1)} %bitcast.159), calls=%async_computation | async-start | bytes 1048576 | tf_op jit(solution)/shard_map/all_to_all | solution.py:126
  118.5 1.2 reduce-window.26
  120.7 2.4 scatter_custom_fusion
  123.1 3.8 %scatter_custom_fusion.1 = bf16[768]{0:T(1024)(128)(2,1)S(1)} fusion(s32[512]{0:T(512)S(1)} %bitcast.173, bf16[512]{0:T(512)(128)(2,1)S(1)} %broadcast.147, bf16[]{:T(256)} %constant.106.clone.1), kind=kCustom, calls=%fused_computation.116 | custom fusion | bytes 1538 | tf_op jit(solution)/shard_map/scatter | solution.py:154
  127.0 20.6 %all-to-all-done = bf16[8,256,128]{2,1,0:T(8,128)(2,1)S(1)} async-done(((bf16[8,256,128]{2,1,0:T(8,128)(2,1)}), bf16[8,256,128]{2,1,0:T(8,128)(2,1)S(1)}, u32[]{:S(2)}, u32[]{:S(2)}) %all-to-all-start) | async-done | bytes 524320 | tf_op jit(solution)/shard_map/all_to_all | solution.py:126
  147.9 4.0 %fusion.46 = (f32[256]{0:T(256)S(1)}, bf16[256,2048]{1,0:T(8,128)(2,1)S(1)}) fusion(bf16[256,1024]{0,1:T(8,128)(2,1)S(1)} %bitcast.163, bf16[1024,2048]{1,0:T(8,128)(2,1)} %all-gather.7.cloned.1.call-done, bf16[256,2048]{1,0:T(8,128)(2,1)} %param.26), kind=kOutput, calls=%fused_computation.66 | convolution fusion | flops 1076887296 | bytes 6816768 | tf_op jit(solution)/shard_map/dot_general | solution.py:127
  151.9 1.0 copy-done.1
  153.2 4.3 %gather_fusion = bf16[768,2048]{1,0:T(8,128)(2,1)} fusion(bf16[256,2048]{1,0:T(8,128)(2,1)S(1)} %fusion.48, s32[1024]{0:T(1024)S(1)} %pad_clamp_fusion.1), kind=kCustom, calls=%fused_computation | custom fusion | bytes 6294528 | tf_op jit(solution)/shard_map/gather | solution.py:155
  157.5 3.8 %broadcast_multiply_fusion = bf16[4,192,2048]{2,1,0:T(8,128)(2,1)} fusion(bf16[4,192,2048]{2,1,0:T(8,128)(2,1)} %bitcast.156, bf16[4,192]{1,0:T(4,128)(2,1)S(1)} %mul.185), kind=kLoop, calls=%fused_computation.69 | loop fusion | flops 1572864 | bytes 6292992 | tf_op jit(solution)/shard_map/mul | solution.py:155
  161.3 4.7 %all-to-all-start.1 = ((bf16[4,192,2048]{2,1,0:T(8,128)(2,1)}), bf16[4,192,2048]{2,1,0:T(8,128)(2,1)}, u32[]{:S(2)}, u32[]{:S(2)}) async-start(bf16[4,192,2048]{2,1,0:T(8,128)(2,1)} %broadcast_multiply_fusion), calls=%async_computation.1 | async-start | bytes 6291456 | tf_op jit(solution)/shard_map/all_to_all | solution.py:158
  166.1 36.7 %all-to-all-done.1 = bf16[4,192,2048]{2,1,0:T(8,128)(2,1)} async-done(((bf16[4,192,2048]{2,1,0:T(8,128)(2,1)}), bf16[4,192,2048]{2,1,0:T(8,128)(2,1)}, u32[]{:S(2)}, u32[]{:S(2)}) %all-to-all-start.1) | async-done | bytes 3145760 | tf_op jit(solution)/shard_map/all_to_all | solution.py:158
  202.7 8.3 %fusion.78 = f32[768,1024]{1,0:T(8,128)} fusion(bf16[768,2048]{1,0:T(8,128)(2,1)} %bitcast.16, bf16[2048,1024]{1,0:T(8,128)(2,1)} %all-gather.9.cloned.1.call-done), kind=kOutput, calls=%fused_computation.125 | convolution fusion | flops 3221225472 | bytes 10485760 | tf_op jit(solution)/shard_map/dot_general | solution.py:161
  211.0 3.9 %all-gather.13.cloned.1.call-done = bf16[2048,1024]{1,0:T(8,128)(2,1)} async-done(((bf16[2048,128]{1,0:T(8,128)(2,1)}), bf16[2048,1024]{1,0:T(8,128)(2,1)}) %all-gather.13.cloned.1.call-update) | async-done | bytes 4194320 | tf_op jit(solution)/shard_map/all_gather | solution.py:105
  214.9 12.5 %convolution_convert_fusion = bf16[768,2048]{1,0:T(8,128)(2,1)} fusion(bf16[2048,1024]{1,0:T(8,128)(2,1)} %all-gather.13.cloned.1.call-done, f32[768,1024]{1,0:T(8,128)} %fusion.78, bf16[768,2048]{1,0:T(8,128)(2,1)} %bitcast.16, bf16[2048,1024]{1,0:T(8,128)(2,1)} %all-gather.11.cloned.1.call-done), kind=kOutput, calls=%fused_computation.54 | convolution fusion | flops 6448742400 | bytes 17825792 | tf_op jit(solution)/shard_map/dot_general | solution.py:164
  227.5 5.0 %all-to-all-start.2 = ((bf16[4,192,2048]{2,1,0:T(8,128)(2,1)}), bf16[4,192,2048]{2,1,0:T(8,128)(2,1)}, u32[]{:S(2)}, u32[]{:S(2)}) async-start(bf16[4,192,2048]{2,1,0:T(8,128)(2,1)} %bitcast.158), calls=%async_computation.2 | async-start | bytes 6291456 | tf_op jit(solution)/shard_map/all_to_all | solution.py:168
  232.7 3.2 %fusion.76 = f32[256,512]{1,0:T(8,128)} fusion(bf16[2048,512]{1,0:T(8,128)(2,1)} %param.35, bf16[256,2048]{1,0:T(8,128)(2,1)S(1)} %copy-done.2, f32[2048]{0:T(1024)S(1)} %copy-done.5, f32[256]{0:T(256)S(1)} %add_rsqrt_fusion.1), kind=kOutput, calls=%fused_computation.124 | convolution fusion | flops 538968064 | bytes 3679232 | tf_op jit(solution)/shard_map/dot_general | solution.py:136
  235.8 33.3 %all-to-all-done.2 = bf16[4,192,2048]{2,1,0:T(8,128)(2,1)} async-done(((bf16[4,192,2048]{2,1,0:T(8,128)(2,1)}), bf16[4,192,2048]{2,1,0:T(8,128)(2,1)}, u32[]{:S(2)}, u32[]{:S(2)}) %all-to-all-start.2) | async-done | bytes 3145760 | tf_op jit(solution)/shard_map/all_to_all | solution.py:168
  269.1 7.6 %gather_fusion.1 = bf16[512,2048]{1,0:T(8,128)(2,1)} fusion(bf16[768,2048]{1,0:T(8,128)(2,1)} %bitcast.18, s32[1024]{0:T(1024)S(1)} %pad_clamp_fusion), kind=kCustom, calls=%fused_computation.1 | custom fusion | bytes 4196352 | tf_op jit(solution)/shard_map/gather | solution.py:169
  276.7 5.4 %reshape.189 = f32[256,2,2048]{2,1,0:T(2,128)} reshape(bf16[512,2048]{1,0:T(8,128)(2,1)} %gather_fusion.1) | data formatting | bytes 6291456 | tf_op jit(solution)/shard_map/convert_element_type | solution.py:169
  282.1 10.1 %multiply_reduce_fusion = f32[256,2048]{1,0:T(8,128)} fusion(f32[256,2,2048]{2,1,0:T(2,128)} %reshape.189, f32[256,2]{1,0:T(8,128)S(1)} %copy.78), kind=kLoop, calls=%fused_computation.53 | loop fusion | flops 1572864 | bytes 6293504 | tf_op jit(solution)/shard_map/reduce_sum | solution.py:171
  292.3 4.8 %fusion.42 = bf16[256,2048]{1,0:T(8,128)(2,1)} fusion(bf16[2048,512]{1,0:T(8,128)(2,1)S(1)} %copy-done, f32[256,2048]{1,0:T(8,128)} %multiply_reduce_fusion, bf16[256,2048]{1,0:T(8,128)(2,1)S(1)} %copy-done.2, bf16[2048,512]{1,0:T(8,128)(2,1)} %param.36, f32[256,512]{1,0:T(8,128)} %fusion.76, f32[2048]{0:T(1024)S(1)} %copy-done.5, f32[256]{0:T(256)S(1)} %add_rsqrt_fusion.1), kind=kOutput, calls=%fused_computation.61 | convolution fusion | flops 1078722560 | bytes 8922112 | tf_op jit(solution)/shard_map/dot_general | solution.py:139
  (118 shorter events, 9.8 us)
Async XLA Ops:
  6.5 285.7 %copy-start = (bf16[2048,512]{1,0:T(8,128)(2,1)S(1)}, bf16[2048,512]{1,0:T(8,128)(2,1)}, u32[]{:S(2)}) copy-start(bf16[2048,512]{1,0:T(8,128)(2,1)} %param.37) | copy-start | bytes 6291460
  6.5 7.1 %copy-start.9 = (u32[32]{0:T(128)S(1)}, u32[32]{0:T(128)}, u32[]{:S(2)}) copy-start(u32[32]{0:T(128)} %constant.111) | copy-start | bytes 388
  6.5 2.8 copy-start.3
  6.5 141.3 %all-gather.7.cloned.1.call-start = ((), (), s32[]{:S(2)}) async-start(), calls=%async_computation.3 | async-start | bytes 4718592 | tf_op jit(solution)/shard_map/all_gather | solution.py:102
  7.3 158.8 %all-gather.9.cloned.1.call-start = ((), (), s32[]{:S(2)}) async-start(), calls=%async_computation.4 | async-start | bytes 4718592 | tf_op jit(solution)/shard_map/all_gather | solution.py:103
  8.0 203.0 %all-gather.11.cloned.1.call-start = ((), (), s32[]{:S(2)}) async-start(), calls=%async_computation.5 | async-start | bytes 4718592 | tf_op jit(solution)/shard_map/all_gather | solution.py:104
  8.7 206.2 %all-gather.13.cloned.1.call-start = ((), (), s32[]{:S(2)}) async-start(), calls=%async_computation.6 | async-start | bytes 4718592 | tf_op jit(solution)/shard_map/all_gather | solution.py:105
  94.3 12.3 %copy-start.4 = (f32[2048,2]{0,1:T(2,128)S(1)}, f32[2048,2]{0,1:T(2,128)}, u32[]{:S(2)}) copy-start(f32[2048,2]{0,1:T(2,128)} %exponential_bitcast_fusion.1) | copy-start | bytes 49156
  108.5 2.7 copy-start.8
  111.2 7.0 %copy-start.6 = (s32[256,2]{0,1:T(2,128)S(1)}, s32[256,2]{0,1:T(2,128)}, u32[]{:S(2)}) copy-start(s32[256,2]{0,1:T(2,128)} %param.30) | copy-start | bytes 6148
  113.3 34.3 %all-to-all-start = ((bf16[8,256,128]{2,1,0:T(8,128)(2,1)}), bf16[8,256,128]{2,1,0:T(8,128)(2,1)S(1)}, u32[]{:S(2)}, u32[]{:S(2)}) async-start(bf16[8,256,128]{2,1,0:T(8,128)(2,1)} %bitcast.159), calls=%async_computation | async-start | bytes 1048576 | tf_op jit(solution)/shard_map/all_to_all | solution.py:126
  147.9 5.0 %copy-start.5 = (f32[2048]{0:T(1024)S(1)}, f32[2048]{0:T(1024)}, u32[]{:S(2)}) copy-start(f32[2048]{0:T(1024)} %param.29) | copy-start | bytes 24580
  151.9 1.0 copy-start.1
  161.3 41.4 %all-to-all-start.1 = ((bf16[4,192,2048]{2,1,0:T(8,128)(2,1)}), bf16[4,192,2048]{2,1,0:T(8,128)(2,1)}, u32[]{:S(2)}, u32[]{:S(2)}) async-start(bf16[4,192,2048]{2,1,0:T(8,128)(2,1)} %broadcast_multiply_fusion), calls=%async_computation.1 | async-start | bytes 6291456 | tf_op jit(solution)/shard_map/all_to_all | solution.py:158
  227.5 5.0 %copy-start.7 = (f32[256,2]{0,1:T(2,128)S(1)}, f32[256,2]{0,1:T(2,128)}, u32[]{:S(2)}) copy-start(f32[256,2]{0,1:T(2,128)} %param.31) | copy-start | bytes 6148
  227.5 5.2 %copy-start.2 = (bf16[256,2048]{1,0:T(8,128)(2,1)S(1)}, bf16[256,2048]{1,0:T(8,128)(2,1)}, u32[]{:S(2)}) copy-start(bf16[256,2048]{1,0:T(8,128)(2,1)} %copy-done.1) | copy-start | bytes 3145732
  227.5 41.6 %all-to-all-start.2 = ((bf16[4,192,2048]{2,1,0:T(8,128)(2,1)}), bf16[4,192,2048]{2,1,0:T(8,128)(2,1)}, u32[]{:S(2)}, u32[]{:S(2)}) async-start(bf16[4,192,2048]{2,1,0:T(8,128)(2,1)} %bitcast.158), calls=%async_computation.2 | async-start | bytes 6291456 | tf_op jit(solution)/shard_map/all_to_all | solution.py:168
Sparse Core Ops, SparseCore 0:
  8.9 50.5 all-gather.6
  61.1 45.9 all-gather.8
  108.8 58.4 all-gather.10
  168.7 46.2 all-gather.12
where the time goes:
time: 305 us; the launch traced here: 304 us
  waiting for transfers between devices  97.1 us (32%)
  local copies, waits for them, and re-layouts  80.6 us (26%)
  matrix products  53 us (17%)
  other arithmetic  24.5 us (8%)
  blocking collectives  19.4 us (6%)
  starting transfers between devices  14.6 us (5%)
  between operations  14.1 us (5%)
    all_to_all x1, waiting for transfers between devices, on_device(): lax.all_to_all(outgoing, 'sp', split_axis=0, concat_axis=0, tiled=True)  36.7 us
    all_to_all x1, waiting for transfers between devices, on_device(): lax.all_to_all(processed, 'sp', split_axis=0, concat_axis=0, tiled=True)  33.3 us
    dynamic_update_slice x8, local copies, waits for them, and re-layouts, block_pass(): lax.scan(advance, state, (query_blocks, key_blocks, value_blocks, decay_b...  25.7 us
    all_to_all x1, waiting for transfers between devices, on_device(): lax.all_to_all(ret_rows, 'tp', split_axis=0, concat_axis=1, tiled=True)  20.6 us
    unnamed x32, local copies, waits for them, and re-layouts  13 us
    dot_general x1, matrix products, on_device(): lax.dot_general(middle, down_full, (((1,), (1,)), ((), ())), preferred_el...  12.5 us
    unnamed x1, blocking collectives  11.4 us
    reduce_sum x1, other arithmetic, on_device(): jnp.sum(decay_weighted.reshape(token_count, chosen_count, model_width), a...  10.1 us
  transfers between devices with their start and end apart: 7, of which 4 were waited for; matrix products, arithmetic and copies ran while one was open for 38% of the time, Pallas kernels for 0%

commit v1 on v0

--- a/solution.py
+++ b/solution.py
@@ -123,7 +123,10 @@
         * head_gain
         * jax.nn.silu(gate_rows.astype(jnp.float32))
     ).astype(jnp.bfloat16)
-    token_rows = lax.all_to_all(ret_rows, "tp", split_axis=0, concat_axis=1, tiled=True)
+    token_rows = jnp.concatenate(
+        lax.all_to_all(jnp.stack(jnp.split(ret_rows, lax.axis_size("tp"), axis=0)), "tp", 0, 0),
+        axis=1,
+    )
     mixer = jnp.dot(token_rows, out_full, preferred_element_type=jnp.float32)
     hidden = (residual.astype(jnp.float32) + mixer).astype(jnp.bfloat16)
     hidden_wide = hidden.astype(jnp.float32)

time: 305 us -> 305 us (level)
  local copies, waits for them, and re-layouts: 80.6 us -> 86 us
  waiting for transfers between devices: 97.1 us -> 92.8 us
    unnamed x32 -> x40, local copies, waits for them, and re-layouts: 13 us -> 19.5 us
  transfers between devices with their start and end apart: 7 -> 7, of which waited for: 4 -> 4; matrix products, arithmetic and copies ran while one was open for 38% -> 40% of each run, Pallas kernels for 0% -> 0%
where the time goes in v1:
time: 305 us; the launch traced here: 303 us
  waiting for transfers between devices  92.8 us (30%)
  local copies, waits for them, and re-layouts  86 us (28%)
  matrix products  52.8 us (17%)
  other arithmetic  23 us (8%)
  blocking collectives  19.4 us (6%)
  starting transfers between devices  14.6 us (5%)
  between operations  14.1 us (5%)
    all_to_all x1, waiting for transfers between devices, on_device(): lax.all_to_all(outgoing, 'sp', split_axis=0, concat_axis=0, tiled=True)  36.1 us
    all_to_all x1, waiting for transfers between devices, on_device(): lax.all_to_all(processed, 'sp', split_axis=0, concat_axis=0, tiled=True)  33.3 us
    dynamic_update_slice x8, local copies, waits for them, and re-layouts, block_pass(): lax.scan(advance, state, (query_blocks, key_blocks, value_blocks, decay_b...  25.7 us
    unnamed x40, local copies, waits for them, and re-layouts  19.5 us
    all_to_all x1, waiting for transfers between devices, on_device(): lax.all_to_all(jnp.stack(jnp.split(ret_rows, lax.axis_size('tp'), axis=0)...  18.3 us
    dot_general x1, matrix products, on_device(): lax.dot_general(middle, down_full, (((1,), (1,)), ((), ())), preferred_el...  12.5 us
    unnamed x1, blocking collectives  11.4 us
    reduce_sum x1, other arithmetic, on_device(): jnp.sum(decay_weighted.reshape(token_count, chosen_count, model_width), a...  10.1 us
  transfers between devices with their start and end apart: 7, of which 4 were waited for; matrix products, arithmetic and copies ran while one was open for 40% of the time, Pallas kernels for 0%

profile of v1, /device:TPU:0, one launch (start us, length us, event | category | flops | bytes accessed | tf_op | source)
XLA Modules:
  0.0 302.9 jit_solution(1000893558062869301)
XLA Ops:
  6.5 0.7 all-gather.7.cloned.1.call-update
  7.3 0.7 all-gather.9.cloned.1.call-update
  8.1 0.7 all-gather.11.cloned.1.call-update
  11.2 2.4 reshape.240
  15.0 2.1 copy.53
  17.1 11.4 %all-reduce = f32[8]{0:T(128)S(1)} all-reduce(f32[8]{0:T(128)S(1)} %bitcast_dynamic-update-slice_fusion), channel_id=2, replica_groups=mesh['sp'=4,'tp'=8] {'sp'}, use_global_device_ids=true, to_apply=%add | all-reduce | flops 8 | bytes 64
  28.4 0.7 reshape.227
  29.1 3.2 %reshape.238 = bf16[4,512,2,64]{3,2,1,0:T(2,128)(2,1)} reshape(bf16[2048,128]{1,0:T(8,128)(2,1)} %param.22) | data formatting | bytes 1048576 | tf_op jit(solution)/shard_map/reshape;reshape | solution.py:30
  32.3 3.5 %copy.48 = bf16[4,512,2,64]{1,3,2,0:T(8,128)(2,1)} copy(bf16[4,512,2,64]{3,2,1,0:T(2,128)(2,1)} %reshape.238) | data formatting | bytes 1048576
  35.8 3.2 %reshape.239 = bf16[4,512,2,64]{3,2,1,0:T(2,128)(2,1)} reshape(bf16[2048,128]{1,0:T(8,128)(2,1)} %param.23) | data formatting | bytes 1048576 | tf_op jit(solution)/shard_map/reshape;reshape | solution.py:31
  39.0 3.5 %copy.49 = bf16[4,512,2,64]{1,3,2,0:T(8,128)(2,1)} copy(bf16[4,512,2,64]{3,2,1,0:T(2,128)(2,1)} %reshape.239) | data formatting | bytes 1048576
  42.5 1.8 copy.50
  44.3 50.0 %while.27 = (s32[]{:T(128)}, f32[2,64,64]{2,1,0:T(8,128)S(1)}, f32[4,512,2,64]{1,0,3,2:T(4,128)}, f32[4,2,512]{2,1,0:T(2,128)S(1)}, bf16[4,512,2,64]{1,3,2,0:T(8...) while((s32[]{:T(128)}, f32[2,64,64]{2,1,0:T(8,128)S(1)}, ...), condition=%wide.region_3.4_spmd.clone, body=%wide.region_0.3_spmd.clone.sunk | while | flops 238192672 | bytes 3317096 | solution.py:65
  45.7 2.1 fusion.116
  47.8 1.2 fusion.117
  49.3 6.2 %dynamic_update_slice.6 = f32[4,512,2,64]{1,0,3,2:T(4,128)} dynamic-update-slice(f32[4,512,2,64]{1,0,3,2:T(4,128)} %get-tuple-element.323, f32[1,512,2,64]{1,0,3,2:T(1,128)S(1)} %copy.103, s32[]{:T(128)} %get-tuple-element.321, s32[]{:T(128)} %constant.94.clone.1..sunk, s32[]{:T(128)} %constant.94.clone.1..sunk, s32[]{:T(128)} %constant.94.clone.1..sunk) | dynamic-update-slice | bytes 524292 | tf_op jit(solution)/shard_map/while/body/jit(dynamic_update_index_in_dim)/dynamic_update_slice | solution.py:65
  55.5 1.2 convolution_add_fusion.4
  58.2 2.2 fusion.116
  60.4 1.2 fusion.117
  61.9 6.2 %dynamic_update_slice.6 = f32[4,512,2,64]{1,0,3,2:T(4,128)} dynamic-update-slice(f32[4,512,2,64]{1,0,3,2:T(4,128)} %get-tuple-element.323, f32[1,512,2,64]{1,0,3,2:T(1,128)S(1)} %copy.103, s32[]{:T(128)} %get-tuple-element.321, s32[]{:T(128)} %constant.94.clone.1..sunk, s32[]{:T(128)} %constant.94.clone.1..sunk, s32[]{:T(128)} %constant.94.clone.1..sunk) | dynamic-update-slice | bytes 524292 | tf_op jit(solution)/shard_map/while/body/jit(dynamic_update_index_in_dim)/dynamic_update_slice | solution.py:65
  68.1 1.3 convolution_add_fusion.4
  70.7 2.1 fusion.116
  72.9 1.2 fusion.117
  74.4 6.1 %dynamic_update_slice.6 = f32[4,512,2,64]{1,0,3,2:T(4,128)} dynamic-update-slice(f32[4,512,2,64]{1,0,3,2:T(4,128)} %get-tuple-element.323, f32[1,512,2,64]{1,0,3,2:T(1,128)S(1)} %copy.103, s32[]{:T(128)} %get-tuple-element.321, s32[]{:T(128)} %constant.94.clone.1..sunk, s32[]{:T(128)} %constant.94.clone.1..sunk, s32[]{:T(128)} %constant.94.clone.1..sunk) | dynamic-update-slice | bytes 524292 | tf_op jit(solution)/shard_map/while/body/jit(dynamic_update_index_in_dim)/dynamic_update_slice | solution.py:65
  80.5 1.2 convolution_add_fusion.4
  83.2 2.1 fusion.116
  85.3 1.2 fusion.117
  86.9 6.1 %dynamic_update_slice.6 = f32[4,512,2,64]{1,0,3,2:T(4,128)} dynamic-update-slice(f32[4,512,2,64]{1,0,3,2:T(4,128)} %get-tuple-element.323, f32[1,512,2,64]{1,0,3,2:T(1,128)S(1)} %copy.103, s32[]{:T(128)} %get-tuple-element.321, s32[]{:T(128)} %constant.94.clone.1..sunk, s32[]{:T(128)} %constant.94.clone.1..sunk, s32[]{:T(128)} %constant.94.clone.1..sunk) | dynamic-update-slice | bytes 524292 | tf_op jit(solution)/shard_map/while/body/jit(dynamic_update_index_in_dim)/dynamic_update_slice | solution.py:65
  93.0 1.2 convolution_add_fusion.4
  94.3 8.0 %all-gather.1 = f32[8,64,64]{2,1,0:T(8,128)S(1)} all-gather(f32[2,64,64]{2,1,0:T(8,128)S(1)} %get-tuple-element.143), channel_id=3, replica_groups=mesh['sp'=4,'tp'=8] {'sp'}, dimensions={0}, use_global_device_ids=true | all-gather | bytes 163840 | tf_op jit(solution)/shard_map/all_gather | solution.py:13
  102.3 2.3 while.28
  102.3 0.7 dynamic-slice_bitcast_fusion.2
  103.1 0.7 dynamic-slice_bitcast_fusion.2
  103.8 0.7 dynamic-slice_bitcast_fusion.2
  104.6 1.9 reshape.183
  106.5 1.7 fusion.81
  108.6 2.0 copy.55
  110.7 1.4 fusion.54
  112.1 0.6 fusion.68
  112.8 0.6 fusion.67
  113.4 0.6 fusion.66
  114.0 0.6 fusion.65
  114.7 0.6 fusion.64
  117.2 4.8 %all-to-all-start = ((bf16[8,256,128]{1,2,0:T(8,128)(2,1)}), bf16[8,256,128]{1,2,0:T(8,128)(2,1)S(1)}, u32[]{:S(2)}, u32[]{:S(2)}) async-start(bf16[8,256,128]{1,2,0:T(8,128)(2,1)} %fusion.61), calls=%async_computation | async-start | bytes 1048576 | tf_op jit(solution)/shard_map/all_to_all | solution.py:127
  122.4 1.2 reduce-window.26
  124.6 2.4 scatter_custom_fusion
  127.0 3.8 %scatter_custom_fusion.1 = bf16[768]{0:T(1024)(128)(2,1)S(1)} fusion(s32[512]{0:T(512)S(1)} %bitcast.207, bf16[512]{0:T(512)(128)(2,1)S(1)} %broadcast.147, bf16[]{:T(256)} %constant.106.clone.1), kind=kCustom, calls=%fused_computation.133 | custom fusion | bytes 1538 | tf_op jit(solution)/shard_map/scatter | solution.py:157
  130.9 18.3 %all-to-all-done = bf16[8,256,128]{1,2,0:T(8,128)(2,1)S(1)} async-done(((bf16[8,256,128]{1,2,0:T(8,128)(2,1)}), bf16[8,256,128]{1,2,0:T(8,128)(2,1)S(1)}, u32[]{:S(2)}, u32[]{:S(2)}) %all-to-all-start) | async-done | bytes 524320 | tf_op jit(solution)/shard_map/all_to_all | solution.py:127
  149.2 3.9 %fusion.46 = (f32[256]{0:T(256)S(1)}, bf16[256,2048]{1,0:T(8,128)(2,1)S(1)}) fusion(bf16[256,1024]{0,1:T(8,128)(2,1)S(1)} %bitcast.197, bf16[1024,2048]{1,0:T(8,128)(2,1)} %all-gather.7.cloned.1.call-done, bf16[256,2048]{1,0:T(8,128)(2,1)} %param.26), kind=kOutput, calls=%fused_computation.66 | convolution fusion | flops 1076887296 | bytes 6816768 | tf_op jit(solution)/shard_map/dot_general | solution.py:130
  153.1 1.0 copy-done.1
  154.4 4.3 %gather_fusion = bf16[768,2048]{1,0:T(8,128)(2,1)} fusion(bf16[256,2048]{1,0:T(8,128)(2,1)S(1)} %fusion.48, s32[1024]{0:T(1024)S(1)} %pad_clamp_fusion.1), kind=kCustom, calls=%fused_computation | custom fusion | bytes 6294528 | tf_op jit(solution)/shard_map/gather | solution.py:158
  158.7 4.0 %broadcast_multiply_fusion = bf16[4,192,2048]{2,1,0:T(8,128)(2,1)} fusion(bf16[4,192,2048]{2,1,0:T(8,128)(2,1)} %bitcast.193, bf16[4,192]{1,0:T(4,128)(2,1)S(1)} %mul.185), kind=kLoop, calls=%fused_computation.69 | loop fusion | flops 1572864 | bytes 6292992 | tf_op jit(solution)/shard_map/mul | solution.py:158
  162.7 4.7 %all-to-all-start.1 = ((bf16[4,192,2048]{2,1,0:T(8,128)(2,1)}), bf16[4,192,2048]{2,1,0:T(8,128)(2,1)}, u32[]{:S(2)}, u32[]{:S(2)}) async-start(bf16[4,192,2048]{2,1,0:T(8,128)(2,1)} %broadcast_multiply_fusion), calls=%async_computation.1 | async-start | bytes 6291456 | tf_op jit(solution)/shard_map/all_to_all | solution.py:161
  167.4 36.1 %all-to-all-done.1 = bf16[4,192,2048]{2,1,0:T(8,128)(2,1)} async-done(((bf16[4,192,2048]{2,1,0:T(8,128)(2,1)}), bf16[4,192,2048]{2,1,0:T(8,128)(2,1)}, u32[]{:S(2)}, u32[]{:S(2)}) %all-to-all-start.1) | async-done | bytes 3145760 | tf_op jit(solution)/shard_map/all_to_all | solution.py:161
  203.6 8.2 %fusion.86 = f32[768,1024]{1,0:T(8,128)} fusion(bf16[768,2048]{1,0:T(8,128)(2,1)} %bitcast.23, bf16[2048,1024]{1,0:T(8,128)(2,1)} %all-gather.9.cloned.1.call-done), kind=kOutput, calls=%fused_computation.142 | convolution fusion | flops 3221225472 | bytes 10485760 | tf_op jit(solution)/shard_map/dot_general | solution.py:164
  211.8 2.5 all-gather.13.cloned.1.call-done
  214.3 12.5 %convolution_convert_fusion = bf16[768,2048]{1,0:T(8,128)(2,1)} fusion(bf16[2048,1024]{1,0:T(8,128)(2,1)} %all-gather.13.cloned.1.call-done, f32[768,1024]{1,0:T(8,128)} %fusion.86, bf16[768,2048]{1,0:T(8,128)(2,1)} %bitcast.23, bf16[2048,1024]{1,0:T(8,128)(2,1)} %all-gather.11.cloned.1.call-done), kind=kOutput, calls=%fused_computation.54 | convolution fusion | flops 6448742400 | bytes 17825792 | tf_op jit(solution)/shard_map/dot_general | solution.py:167
  226.8 5.0 %all-to-all-start.2 = ((bf16[4,192,2048]{2,1,0:T(8,128)(2,1)}), bf16[4,192,2048]{2,1,0:T(8,128)(2,1)}, u32[]{:S(2)}, u32[]{:S(2)}) async-start(bf16[4,192,2048]{2,1,0:T(8,128)(2,1)} %bitcast.194), calls=%async_computation.2 | async-start | bytes 6291456 | tf_op jit(solution)/shard_map/all_to_all | solution.py:171
  232.0 3.2 %fusion.84 = f32[256,512]{1,0:T(8,128)} fusion(bf16[2048,512]{1,0:T(8,128)(2,1)} %param.35, bf16[256,2048]{1,0:T(8,128)(2,1)S(1)} %copy-done.2, f32[2048]{0:T(1024)S(1)} %copy-done.5, f32[256]{0:T(256)S(1)} %add_rsqrt_fusion.1), kind=kOutput, calls=%fused_computation.141 | convolution fusion | flops 538968064 | bytes 3679232 | tf_op jit(solution)/shard_map/dot_general | solution.py:139
  235.1 33.3 %all-to-all-done.2 = bf16[4,192,2048]{2,1,0:T(8,128)(2,1)} async-done(((bf16[4,192,2048]{2,1,0:T(8,128)(2,1)}), bf16[4,192,2048]{2,1,0:T(8,128)(2,1)}, u32[]{:S(2)}, u32[]{:S(2)}) %all-to-all-start.2) | async-done | bytes 3145760 | tf_op jit(solution)/shard_map/all_to_all | solution.py:171
  268.5 7.6 %gather_fusion.1 = bf16[512,2048]{1,0:T(8,128)(2,1)} fusion(bf16[768,2048]{1,0:T(8,128)(2,1)} %bitcast.25, s32[1024]{0:T(1024)S(1)} %pad_clamp_fusion), kind=kCustom, calls=%fused_computation.1 | custom fusion | bytes 4196352 | tf_op jit(solution)/shard_map/gather | solution.py:172
  276.0 5.4 %reshape.194 = f32[256,2,2048]{2,1,0:T(2,128)} reshape(bf16[512,2048]{1,0:T(8,128)(2,1)} %gather_fusion.1) | data formatting | bytes 6291456 | tf_op jit(solution)/shard_map/convert_element_type | solution.py:172
  281.5 10.1 %multiply_reduce_fusion = f32[256,2048]{1,0:T(8,128)} fusion(f32[256,2,2048]{2,1,0:T(2,128)} %reshape.194, f32[256,2]{1,0:T(8,128)S(1)} %copy.59), kind=kLoop, calls=%fused_computation.53 | loop fusion | flops 1572864 | bytes 6293504 | tf_op jit(solution)/shard_map/reduce_sum | solution.py:174
  291.6 4.8 %fusion.42 = bf16[256,2048]{1,0:T(8,128)(2,1)} fusion(bf16[2048,512]{1,0:T(8,128)(2,1)S(1)} %copy-done, f32[256,2048]{1,0:T(8,128)} %multiply_reduce_fusion, bf16[256,2048]{1,0:T(8,128)(2,1)S(1)} %copy-done.2, bf16[2048,512]{1,0:T(8,128)(2,1)} %param.36, f32[256,512]{1,0:T(8,128)} %fusion.84, f32[2048]{0:T(1024)S(1)} %copy-done.5, f32[256]{0:T(256)S(1)} %add_rsqrt_fusion.1), kind=kOutput, calls=%fused_computation.61 | convolution fusion | flops 1078722560 | bytes 8922112 | tf_op jit(solution)/shard_map/dot_general | solution.py:142
  (125 shorter events, 14.1 us)
Async XLA Ops:
  6.5 285.0 %copy-start = (bf16[2048,512]{1,0:T(8,128)(2,1)S(1)}, bf16[2048,512]{1,0:T(8,128)(2,1)}, u32[]{:S(2)}) copy-start(bf16[2048,512]{1,0:T(8,128)(2,1)} %param.37) | copy-start | bytes 6291460
  6.5 7.1 %copy-start.9 = (u32[32]{0:T(128)S(1)}, u32[32]{0:T(128)}, u32[]{:S(2)}) copy-start(u32[32]{0:T(128)} %constant.111) | copy-start | bytes 388
  6.5 2.8 copy-start.3
  6.5 142.6 %all-gather.7.cloned.1.call-start = ((), (), s32[]{:S(2)}) async-start(), calls=%async_computation.3 | async-start | bytes 4718592 | tf_op jit(solution)/shard_map/all_gather | solution.py:102
  7.3 160.2 %all-gather.9.cloned.1.call-start = ((), (), s32[]{:S(2)}) async-start(), calls=%async_computation.4 | async-start | bytes 4718592 | tf_op jit(solution)/shard_map/all_gather | solution.py:103
  8.0 203.8 %all-gather.11.cloned.1.call-start = ((), (), s32[]{:S(2)}) async-start(), calls=%async_computation.5 | async-start | bytes 4718592 | tf_op jit(solution)/shard_map/all_gather | solution.py:104
  8.7 205.5 %all-gather.13.cloned.1.call-start = ((), (), s32[]{:S(2)}) async-start(), calls=%async_computation.6 | async-start | bytes 4718592 | tf_op jit(solution)/shard_map/all_gather | solution.py:105
  94.3 12.3 %copy-start.4 = (f32[2048,2]{0,1:T(2,128)S(1)}, f32[2048,2]{0,1:T(2,128)}, u32[]{:S(2)}) copy-start(f32[2048,2]{0,1:T(2,128)} %exponential_bitcast_fusion.1) | copy-start | bytes 49156
  108.3 2.4 copy-start.8
  110.7 11.4 %copy-start.6 = (s32[256,2]{0,1:T(2,128)S(1)}, s32[256,2]{0,1:T(2,128)}, u32[]{:S(2)}) copy-start(s32[256,2]{0,1:T(2,128)} %param.30) | copy-start | bytes 6148
  117.2 31.9 %all-to-all-start = ((bf16[8,256,128]{1,2,0:T(8,128)(2,1)}), bf16[8,256,128]{1,2,0:T(8,128)(2,1)S(1)}, u32[]{:S(2)}, u32[]{:S(2)}) async-start(bf16[8,256,128]{1,2,0:T(8,128)(2,1)} %fusion.61), calls=%async_computation | async-start | bytes 1048576 | tf_op jit(solution)/shard_map/all_to_all | solution.py:127
  149.2 4.9 %copy-start.5 = (f32[2048]{0:T(1024)S(1)}, f32[2048]{0:T(1024)}, u32[]{:S(2)}) copy-start(f32[2048]{0:T(1024)} %param.29) | copy-start | bytes 24580
  153.1 1.0 copy-start.1
  162.7 40.9 %all-to-all-start.1 = ((bf16[4,192,2048]{2,1,0:T(8,128)(2,1)}), bf16[4,192,2048]{2,1,0:T(8,128)(2,1)}, u32[]{:S(2)}, u32[]{:S(2)}) async-start(bf16[4,192,2048]{2,1,0:T(8,128)(2,1)} %broadcast_multiply_fusion), calls=%async_computation.1 | async-start | bytes 6291456 | tf_op jit(solution)/shard_map/all_to_all | solution.py:161
  226.8 5.0 %copy-start.7 = (f32[256,2]{0,1:T(2,128)S(1)}, f32[256,2]{0,1:T(2,128)}, u32[]{:S(2)}) copy-start(f32[256,2]{0,1:T(2,128)} %param.31) | copy-start | bytes 6148
  226.8 5.2 %copy-start.2 = (bf16[256,2048]{1,0:T(8,128)(2,1)S(1)}, bf16[256,2048]{1,0:T(8,128)(2,1)}, u32[]{:S(2)}) copy-start(bf16[256,2048]{1,0:T(8,128)(2,1)} %copy-done.1) | copy-start | bytes 3145732
  226.8 41.6 %all-to-all-start.2 = ((bf16[4,192,2048]{2,1,0:T(8,128)(2,1)}), bf16[4,192,2048]{2,1,0:T(8,128)(2,1)}, u32[]{:S(2)}, u32[]{:S(2)}) async-start(bf16[4,192,2048]{2,1,0:T(8,128)(2,1)} %bitcast.194), calls=%async_computation.2 | async-start | bytes 6291456 | tf_op jit(solution)/shard_map/all_to_all | solution.py:171
Sparse Core Ops, SparseCore 0:
  8.9 50.5 all-gather.6
  61.1 45.9 all-gather.8
  108.8 56.5 all-gather.10
  166.8 47.3 all-gather.12
